TPU v7x, 32 devices: a whole 2x2x4 slice. The times are simulated.
32 devices in a mesh: sp: 8 (over z, y), tp: 4 (over x, core).
Axes of the slice: x: 2, y: 2, z: 4, core: 2. Of those that a mesh axis runs over, the one named last changes fastest.
Arguments:
- inputs: bfloat16 [2, 1024, 2048], P(None, 'sp'), may hold values from -6 to 6
- norm_gain: float32 [2048], replicated, may hold values from 0.1 to 1.9
- query_weight: bfloat16 [2048, 1024], P('sp', 'tp'), may hold values from -0.125 to 0.125
- key_weight: bfloat16 [2048, 256], P('sp', 'tp'), may hold values from -0.125 to 0.125
- value_weight: bfloat16 [2048, 256], P('sp', 'tp'), may hold values from -0.125 to 0.125
- query_gain: float32 [64], replicated, may hold values from 0.1 to 24
- key_gain: float32 [64], replicated, may hold values from 0.1 to 1.9
- forget_cache: float32 [2, 16, 1024], P(None, 'tp'), may hold values from -104 to 0, as said below
- rec_in_weight: bfloat16 [2048, 1024], P('sp', 'tp'), may hold values from -0.125 to 0.125
- rec_gate_weight: bfloat16 [2048, 1024], P('sp', 'tp'), may hold values from -0.125 to 0.125
- conv_weight: bfloat16 [4, 1024], P(None, 'tp'), may hold values from -3 to 3
- decay_gate_weight: bfloat16 [16, 64, 64], P('tp'), may hold values from -0.75 to 0.75
- input_gate_weight: bfloat16 [16, 64, 64], P('tp'), may hold values from -0.75 to 0.75
- decay_param: float32 [1024], P('tp'), may hold values from 4 to 16
- decay_extra: float32 [2, 1024, 1024], P(None, 'sp', 'tp'), may hold values from -2 to 0
- attn_out_gain: float32 [1024], P('tp'), may hold values from 0.1 to 1.9
- rec_out_gain: float32 [1024], P('tp'), may hold values from 0.1 to 1.9
- out_att_weight: bfloat16 [1024, 2048], P('tp'), may hold values from -0.125 to 0.125
- out_rec_weight: bfloat16 [1024, 2048], P('tp'), may hold values from -0.125 to 0.125
Outputs:
- mixed: bfloat16 [2, 1024, 2048], P(None, 'sp', 'tp')
Inputs may be any that keep to these rules, and one draw needn't show every extreme that they name: `forget_cache`: Non-increasing along the positions of each sequence and head.
All inputs are finite; a program needn't handle non-finite values.
Results may differ from a plain program's by a relative error of at most 0.012.
The roundings to bfloat16 on the way count: a program that leaves them out, or rounds other values in their place, can miss the bound.
Values may be sent and summed in bfloat16 or wider, within the bound.
A program may use at most 128 MiB of HBM per device.

v0:
```python
import jax
import jax.numpy as jnp
from jax import lax
from jax.sharding import PartitionSpec as P

D = 2048
LRU_BLOCK = 64
CONV_TAPS = 4
lru_const = 8.0
norm_eps = 1e-06


def from_behind(value, axis, steps):
    count = lax.axis_size(axis)
    leading, last = (max(0, -steps), min(count, count - steps))
    return lax.ppermute(value, axis, [(source, source + steps) for source in range(leading, last)])


def rms_scale(values, gain):
    multiplier = lax.rsqrt(jnp.mean(values * values, axis=-1, keepdims=True) + norm_eps)
    return values * multiplier * gain


def merge_state(earlier, later):
    return (earlier[0] * later[0], later[0] * earlier[1] + later[1])


def block_length(length, span):
    shards = max(length // span, 1)
    group_size = 1
    for trial_size in range(1, shards + 1):
        if shards % trial_size == 0 and trial_size * span <= 1024:
            group_size = trial_size
    sub_size = group_size * span
    if length % sub_size:
        sub_size = length
    return sub_size


def body(
    inputs,
    norm_gain,
    query_weight,
    key_weight,
    value_weight,
    query_gain,
    key_gain,
    forget_cache,
    rec_in_weight,
    rec_gate_weight,
    conv_weight,
    decay_gate_weight,
    input_gate_weight,
    decay_param,
    decay_extra,
    attn_out_gain,
    rec_out_gain,
    out_att_weight,
    out_rec_weight,
):
    seq_count, seq_span, model_width = inputs.shape
    row_count = seq_count * seq_span
    head_dim = query_gain.shape[0]
    att_local = query_weight.shape[1] // head_dim
    kv_local = key_weight.shape[1] // head_dim
    head_group = att_local // kv_local
    channels = rec_in_weight.shape[1]
    normed = rms_scale(
        inputs.reshape(row_count, model_width).astype(jnp.float32), norm_gain
    ).astype(jnp.bfloat16)
    normed_cols = normed.T
    row_contract = (((0,), (0,)), ((), ()))
    kv_cols = key_weight.shape[1]
    pieces = (
        lax.all_gather(query_weight, "sp", axis=0, tiled=True),
        lax.all_gather(key_weight, "sp", axis=0, tiled=True),
        lax.all_gather(value_weight, "sp", axis=0, tiled=True),
        lax.all_gather(rec_in_weight, "sp", axis=0, tiled=True),
        lax.all_gather(rec_gate_weight, "sp", axis=0, tiled=True),
    )
    query_proj, key_proj, value_sum, rec_in_sum, gate_proj = tuple(
        (
            lax.dot_general(
                normed_cols, weight_part, row_contract, preferred_element_type=jnp.float32
            )
            for weight_part in pieces
        )
    )
    queries = rms_scale(query_proj.reshape(row_count, att_local, head_dim), query_gain).astype(
        jnp.bfloat16
    )
    queries = queries.reshape(seq_count, seq_span, kv_local, head_group, head_dim).transpose(
        0, 2, 3, 1, 4
    )
    queries = queries.reshape(seq_count, kv_local, head_group * seq_span, head_dim)
    key_heads = rms_scale(key_proj.reshape(row_count, kv_local, head_dim), key_gain).astype(
        jnp.bfloat16
    )
    key_heads = key_heads.reshape(seq_count, seq_span, kv_cols)
    value_heads = value_sum.astype(jnp.bfloat16).reshape(seq_count, seq_span, kv_cols)
    key_value = jnp.concatenate([key_heads, value_heads], axis=2)
    my_first = lax.axis_index("sp") * seq_span
    own_gates = lax.dynamic_slice_in_dim(forget_cache, my_first, seq_span, 2)
    own_gates = own_gates.reshape(seq_count, kv_local, head_group, seq_span, 1)
    query_pos = my_first + jnp.tile(jnp.arange(seq_span, dtype=jnp.int32), head_group)
    scaling = head_dim ** (-0.5)
    start_state = (
        jnp.full((seq_count, kv_local, head_group * seq_span), -jnp.inf, jnp.float32),
        jnp.zeros((seq_count, kv_local, head_group * seq_span), jnp.float32),
        jnp.zeros((seq_count, kv_local, head_group * seq_span, head_dim), jnp.float32),
    )
    shard_part = lax.all_gather(key_value, "sp", axis=1, tiled=True)
    offset = jnp.int32(0)
    length = shard_part.shape[1]
    sub_size = block_length(length, seq_span)

    def one_step(block_index, carried_state):
        key_first = offset + block_index * sub_size

        def work(carried):
            top_score, totals, accum = carried
            block_rows = lax.dynamic_slice_in_dim(shard_part, block_index * sub_size, sub_size, 1)
            key_block = block_rows[:, :, :kv_cols].reshape(seq_count, sub_size, kv_local, head_dim)
            value_block = block_rows[:, :, kv_cols:].reshape(
                seq_count, sub_size, kv_local, head_dim
            )
            key_gates = lax.dynamic_slice_in_dim(forget_cache, key_first, sub_size, 2)
            key_gates = key_gates.reshape(seq_count, kv_local, head_group, 1, sub_size)
            scores = (
                jnp.einsum(
                    "bhqd,bkhd->bhqk", queries, key_block, preferred_element_type=jnp.float32
                )
                * scaling
            )
            scores = (
                scores.reshape(seq_count, kv_local, head_group, seq_span, sub_size)
                + own_gates
                - key_gates
            )
            scores = scores.reshape(seq_count, kv_local, head_group * seq_span, sub_size)
            visible = (
                query_pos[:, None] >= (key_first + jnp.arange(sub_size, dtype=jnp.int32))[None, :]
            )
            scores = jnp.where(visible, scores, -jnp.inf)
            new_top = jnp.maximum(top_score, jnp.max(scores, axis=-1))
            safe_top = jnp.where(jnp.isfinite(new_top), new_top, 0.0)
            weights = jnp.exp(scores - safe_top[..., None])
            fading = jnp.exp(top_score - safe_top)
            totals = totals * fading + jnp.sum(weights, axis=-1)
            accum = accum * fading[..., None] + jnp.einsum(
                "bhqk,bkhd->bhqd",
                weights.astype(jnp.bfloat16),
                value_block,
                preferred_element_type=jnp.float32,
            )
            return (new_top, totals, accum)

        return lax.cond(
            key_first < my_first + seq_span, work, lambda carried: carried, carried_state
        )

    top_score, totals, accum = lax.fori_loop(0, length // sub_size, one_step, start_state)
    attended = (accum / totals[..., None]).reshape(
        seq_count, kv_local, head_group, seq_span, head_dim
    )
    attended = attended.transpose(0, 3, 1, 2, 4).reshape(row_count, att_local, head_dim)
    att_normed = rms_scale(attended, attn_out_gain.reshape(att_local, head_dim)).astype(
        jnp.bfloat16
    )
    att_normed = att_normed.reshape(row_count, att_local * head_dim)
    rec_in = rec_in_sum.astype(jnp.bfloat16).reshape(seq_count, seq_span, channels)
    before = from_behind(rec_in[:, seq_span - (CONV_TAPS - 1) :, :], "sp", 1)
    extended = jnp.concatenate([before, rec_in], axis=1)
    conv = jnp.zeros((seq_count, seq_span, channels), jnp.float32)
    for tap in range(CONV_TAPS):
        conv = conv + extended[:, tap : tap + seq_span].astype(jnp.float32) * conv_weight[
            tap
        ].astype(jnp.float32)
    conv = conv.astype(jnp.bfloat16)
    blocks_local = decay_gate_weight.shape[0]
    grouped = conv.reshape(seq_count, seq_span, blocks_local, LRU_BLOCK)
    gate_decay = jnp.einsum(
        "bsnd,nde->bsne", grouped, decay_gate_weight, preferred_element_type=jnp.float32
    ).reshape(seq_count, seq_span, channels)
    gate_input = jnp.einsum(
        "bsnd,nde->bsne", grouped, input_gate_weight, preferred_element_type=jnp.float32
    ).reshape(seq_count, seq_span, channels)
    log_decay = (
        -lru_const * jax.nn.sigmoid(gate_decay) * jax.nn.softplus(-decay_param) + decay_extra
    )
    drive = (
        jnp.sqrt(-jnp.expm1(2.0 * log_decay))
        * jax.nn.sigmoid(gate_input)
        * conv.astype(jnp.float32)
    )
    cum_decay, local_state = lax.associative_scan(merge_state, (jnp.exp(log_decay), drive), axis=1)
    every_decay, every_state = (
        lax.all_gather(cum_decay[:, seq_span - 1][None], "sp", axis=0, tiled=True),
        lax.all_gather(local_state[:, seq_span - 1][None], "sp", axis=0, tiled=True),
    )
    prefix_decay, prefix_state = lax.associative_scan(
        merge_state, (every_decay, every_state), axis=0
    )
    position = lax.axis_index("sp")
    earlier_state = lax.dynamic_index_in_dim(
        prefix_state, jnp.maximum(position - 1, 0), 0, keepdims=False
    )
    entering = jnp.where(position > 0, earlier_state, 0.0)
    state = local_state + cum_decay * entering[:, None, :]
    gated = state * jax.nn.gelu(gate_proj.reshape(seq_count, seq_span, channels))
    rec_normed = rms_scale(
        gated.reshape(row_count, blocks_local, LRU_BLOCK),
        rec_out_gain.reshape(blocks_local, LRU_BLOCK),
    ).astype(jnp.bfloat16)
    rec_normed = rec_normed.reshape(row_count, channels)
    out_cols = D // lax.axis_size("tp")
    pieces = row_count * lax.axis_size("tp") // row_count
    terms = jnp.dot(att_normed, out_att_weight, preferred_element_type=jnp.float32) + jnp.dot(
        rec_normed, out_rec_weight, preferred_element_type=jnp.float32
    )
    mixed_cols = lax.psum_scatter(
        terms.reshape(row_count, pieces, out_cols)
        .transpose(1, 0, 2)
        .reshape(pieces * row_count, out_cols)
        .astype(jnp.bfloat16),
        "tp",
        scatter_dimension=0,
        tiled=True,
    )
    return mixed_cols.reshape(seq_count, seq_span, out_cols)


def solution(mesh):
    return jax.shard_map(
        body,
        mesh=mesh,
        in_specs=(
            P(None, "sp", None),
            P(),
            P("sp", "tp"),
            P("sp", "tp"),
            P("sp", "tp"),
            P(),
            P(),
            P(None, "tp", None),
            P("sp", "tp"),
            P("sp", "tp"),
            P(None, "tp"),
            P("tp", None, None),
            P("tp", None, None),
            P("tp"),
            P(None, "sp", "tp"),
            P("tp"),
            P("tp"),
            P("tp", None),
            P("tp", None),
        ),
        out_specs=P(None, "sp", "tp"),
        check_vma=False,
    )
```

profile of v0, /device:TPU:0, one launch (start us, length us, event | category | flops | bytes accessed | tf_op | source)
XLA Modules:
  0.0 263.9 jit_solution(10849590766930557368)
XLA Ops:
  9.5 1.5 multiply_reduce_fusion
  11.0 1.4 slice_convert_fusion.3
  12.4 33.4 %all_gather.25 = bf16[2048,64]{0,1:T(8,128)(2,1)S(1)} all-gather(bf16[256,64]{0,1:T(8,128)(2,1)} %param.24), channel_id=1, replica_groups=mesh['sp'=8,'tp'=4] {'sp'}, dimensions={0}, use_global_device_ids=true | all-gather | bytes 294912 | tf_op jit(solution)/shard_map/all_gather | solution.py:76
  45.8 31.4 %all_gather.26 = bf16[2048,64]{0,1:T(8,128)(2,1)S(1)} all-gather(bf16[256,64]{0,1:T(8,128)(2,1)} %param.25), channel_id=1, replica_groups=mesh['sp'=8,'tp'=4] {'sp'}, dimensions={0}, use_global_device_ids=true | all-gather | bytes 294912 | tf_op jit(solution)/shard_map/all_gather | solution.py:77
  77.2 1.0 fusion.14
  79.3 29.7 %all_gather.27 = bf16[2,1024,128]{1,2,0:T(8,128)(2,1)} all-gather(bf16[2,128,128]{1,2,0:T(8,128)(2,1)S(1)} %pad_maximum_fusion.3), channel_id=1, replica_groups=mesh['sp'=8,'tp'=4] {'sp'}, dimensions={1}, use_global_device_ids=true | all-gather | bytes 589824 | tf_op jit(solution)/shard_map/all_gather | solution.py:112
  108.9 1.3 multiply_convert_fusion
  110.3 2.4 copy.49
  112.6 1.7 multiply_reduce_fusion.1
  114.6 6.3 %conditional.1 = ((f32[2,1,512]{2,0,1:T(2,128)S(1)}, f32[2,1,512,64]{2,3,0,1:T(8,128)S(1)})) conditional(s32[]{:T(128)} %convert_element_type.124, (f32[2,1,512]{2,0,1:T(2,128)S(1)}, f32[2,1,512,64]{2,3,0,1:T(8,128)S(1)}) %tuple.30, (s32[]{:T(128)}, s32[4,128]{1,0:T(4,128)S(1)}, bf16[2,1,4,128,64]{3,2,4,0,1:T(4,128)(2,1)S(1)}, ...), branch_computations={%region_3.4_spmd, %region_4.7_spmd} | conditional | flops 281680384 | bytes 17967226 | solution.py:158
  114.7 0.8 dynamic-slice_bitcast_fusion
  115.9 2.4 fusion.3
  118.4 1.8 fusion.1
  120.2 0.8 fusion.4
  121.5 1.7 convolution_convert_fusion
  123.3 3.3 %collective-permute-start = (bf16[2,3,256]{2,1,0:T(4,128)(2,1)S(1)}, bf16[2,3,256]{2,1,0:T(4,128)(2,1)S(1)}, u32[]{:S(2)}, u32[]{:S(2)}) collective-permute-start(bf16[2,3,256]{2,1,0:T(4,128)(2,1)S(1)} %slice.399), channel_id=1, source_target_pairs={{0,4},{4,8},{8,12},{12,16},{16,20},{20,24},{24,28},{1,5},{5,9},{9,... | collective-permute-start | bytes 9224 | tf_op jit(solution)/shard_map/ppermute | solution.py:16
  129.1 0.8 copy.62
  129.9 1.2 fusion.22
  131.1 0.8 copy.58
  132.0 2.0 convert_multiply_fusion
  134.7 1.6 slice.363
  136.4 1.0 slice.317
  137.3 1.6 slice.316
  141.6 1.1 multiply_add_fusion.1
  147.7 0.8 fusion.53
  149.2 0.8 pad.128
  151.9 0.9 pad_maximum_fusion.4
  152.8 2.1 pad.116
  154.9 0.8 pad.130
  155.7 1.6 add.383
  157.3 1.7 fusion.45
  159.0 1.5 pad.117
  160.5 2.3 pad.118
  162.8 0.7 slice_add_fusion.4
  163.6 26.3 %all-gather = f32[16,1,256]{2,1,0:T(1,128)S(1)} all-gather(f32[2,1,256]{2,1,0:T(1,128)S(1)} %slice_add_fusion.4), channel_id=2, replica_groups=mesh['sp'=8,'tp'=4] {'sp'}, dimensions={0}, use_global_device_ids=true | all-gather | bytes 18432 | tf_op jit(solution)/shard_map/all_gather | solution.py:199
  190.4 1.6 pad_maximum_fusion.2
  192.0 0.9 pad.131
  193.6 0.7 reshape.378
  194.3 1.2 copy.63
  195.6 1.4 pad.132
  197.7 26.1 %all-gather.1 = f32[16,1,256]{2,1,0:T(1,128)S(1)} all-gather(f32[2,1,256]{2,1,0:T(1,128)S(1)} %slice_add_fusion.3), channel_id=3, replica_groups=mesh['sp'=8,'tp'=4] {'sp'}, dimensions={0}, use_global_device_ids=true | all-gather | bytes 18432 | tf_op jit(solution)/shard_map/all_gather | solution.py:198
  224.9 3.0 %fusion.73 = (f32[2,128,256]{2,1,0:T(8,128)}, f32[2,128,256]{2,1,0:T(8,128)}) fusion(bf16[2,128,2048]{2,1,0:T(8,128)(2,1)} %multiply_convert_fusion, bf16[2048,256]{1,0:T(8,128)(2,1)} %all-gather.10.cloned.1.call-done, f32[2,256]{1,0:T(2,128)S(1)} %fusion.65, f32[2,128,256]{2,1,0:T(8,128)S(1)} %pad.131, f32[2,128,256]{2,1,0:T(8,128)} %pad.132, ...), kind=kOutput, calls=%fused_computation.170 | convolution fusion | flops 269352960 | bytes 3672064 | tf_op jit(solution)/shard_map/dot_general | solution.py:83
  227.9 1.8 copy.64
  229.7 1.2 mul.431
  230.9 1.1 copy.65
  232.1 1.7 fusion.12
  233.8 1.1 copy.94
  234.9 22.5 %reduce-scatter.2.cloned.1.call-done = bf16[256,512]{1,0:T(8,128)(2,1)} async-done(((bf16[1024,512]{1,0:T(8,128)(2,1)}), bf16[256,512]{1,0:T(8,128)(2,1)}) %reduce-scatter.2.cloned.1.call-update) | async-done | bytes 262160 | tf_op jit(solution)/shard_map/reduce_scatter | solution.py:221
  (192 shorter events, 21.6 us)
Async XLA Ops:
  6.5 120.2 %copy-start = (bf16[256,2048]{1,0:T(8,128)(2,1)S(1)}, bf16[256,2048]{1,0:T(8,128)(2,1)}, u32[]{:S(2)}) copy-start(bf16[256,2048]{1,0:T(8,128)(2,1)} %param.38) | copy-start | bytes 3145732
  6.5 70.7 %copy-start.1 = (bf16[2,128,2048]{2,1,0:T(8,128)(2,1)S(1)}, bf16[2,128,2048]{2,1,0:T(8,128)(2,1)}, u32[]{:S(2)}) copy-start(bf16[2,128,2048]{2,1,0:T(8,128)(2,1)} %param.21) | copy-start | bytes 3145732
  6.5 103.7 %all-gather.6.cloned.1.call-start = ((), (), s32[]{:S(2)}) async-start(), calls=%async_computation.1 | async-start | bytes 1179648 | tf_op jit(solution)/shard_map/all_gather | solution.py:75
  7.3 114.3 %all-gather.8.cloned.1.call-start = ((), (), s32[]{:S(2)}) async-start(), calls=%async_computation.2 | async-start | bytes 1179648 | tf_op jit(solution)/shard_map/all_gather | solution.py:78
  8.0 216.8 %all-gather.10.cloned.1.call-start = ((), (), s32[]{:S(2)}) async-start(), calls=%async_computation.3 | async-start | bytes 1179648 | tf_op jit(solution)/shard_map/all_gather | solution.py:79
  8.7 248.6 %reduce-scatter.2.cloned.1.call-start = ((), (), s32[]{:S(2)}) async-start(), calls=%async_computation.4 | async-start | bytes 1310720 | tf_op jit(solution)/shard_map/reduce_scatter | solution.py:221
  77.2 2.0 copy-start.15
  78.2 30.7 %copy-start.8 = (f32[2048]{0:T(1024)S(1)}, f32[2048]{0:T(1024)}, u32[]{:S(2)}) copy-start(f32[2048]{0:T(1024)} %param.22) | copy-start | bytes 24580
  110.2 2.4 copy-start.2
  112.6 1.7 copy-start.16
  115.9 2.5 copy-start.6
  118.3 1.8 copy-start.3
  121.0 5.6 %copy-start.13 = (f32[256]{0:T(256)S(1)}, f32[256]{0:T(256)}, u32[]{:S(2)}) copy-start(f32[256]{0:T(256)} %param.36) | copy-start | bytes 3076
  123.2 4.6 %copy-start.9 = (f32[1,256]{1,0:T(1,128)S(1)}, f32[1,256]{1,0:T(1,128)}, u32[]{:S(2)}) copy-start(f32[1,256]{1,0:T(1,128)} %get-tuple-element.199) | copy-start | bytes 3076
  123.2 4.6 %copy-start.10 = (f32[1,256]{1,0:T(1,128)S(1)}, f32[1,256]{1,0:T(1,128)}, u32[]{:S(2)}) copy-start(f32[1,256]{1,0:T(1,128)} %get-tuple-element.200) | copy-start | bytes 3076
  123.2 4.6 %copy-start.11 = (f32[1,256]{1,0:T(1,128)S(1)}, f32[1,256]{1,0:T(1,128)}, u32[]{:S(2)}) copy-start(f32[1,256]{1,0:T(1,128)} %get-tuple-element.201) | copy-start | bytes 3076
  123.2 4.6 %copy-start.12 = (f32[1,256]{1,0:T(1,128)S(1)}, f32[1,256]{1,0:T(1,128)}, u32[]{:S(2)}) copy-start(f32[1,256]{1,0:T(1,128)} %get-tuple-element.202) | copy-start | bytes 3076
  123.3 4.6 %collective-permute-start = (bf16[2,3,256]{2,1,0:T(4,128)(2,1)S(1)}, bf16[2,3,256]{2,1,0:T(4,128)(2,1)S(1)}, u32[]{:S(2)}, u32[]{:S(2)}) collective-permute-start(bf16[2,3,256]{2,1,0:T(4,128)(2,1)S(1)} %slice.399), channel_id=1, source_target_pairs={{0,4},{4,8},{8,12},{12,16},{16,20},{20,24},{24,28},{1,5},{5,9},{9,... | collective-permute-start | bytes 9224 | tf_op jit(solution)/shard_map/ppermute | solution.py:16
  126.6 2.2 copy-start.17
  128.1 0.7 copy-start.7
  144.1 7.1 %copy-start.4 = (f32[2,31,256]{2,1,0:T(8,128)S(1)}, f32[2,31,256]{2,1,0:T(8,128)}, u32[]{:S(2)}) copy-start(f32[2,31,256]{2,1,0:T(8,128)} %slice.361) | copy-start | bytes 190468
  144.2 7.1 %copy-start.5 = (f32[2,31,256]{2,1,0:T(8,128)S(1)}, f32[2,31,256]{2,1,0:T(8,128)}, u32[]{:S(2)}) copy-start(f32[2,31,256]{2,1,0:T(8,128)} %slice.320) | copy-start | bytes 190468
  224.8 7.1 %copy-start.14 = (f32[256]{0:T(256)S(1)}, f32[256]{0:T(256)}, u32[]{:S(2)}) copy-start(f32[256]{0:T(256)} %param.37) | copy-start | bytes 3076
Sparse Core Ops, SparseCore 0:
  9.5 44.2 all-gather.5
  55.9 41.5 all-gather.7
  99.6 38.9 all-gather.9
  235.0 22.3 reduce-scatter.1
where the time goes:
time: 265 us; the launch traced here: 264 us
  blocking collectives  147 us (55%)
  local copies, waits for them, and re-layouts  35.4 us (13%)
  waiting for transfers between devices  25.4 us (10%)
  other arithmetic  24.8 us (9%)
  matrix products  14.1 us (5%)
  between operations  13.9 us (5%)
  starting transfers between devices  3.38 us (1%)
    all_gather x1, blocking collectives, body(): lax.all_gather(key_weight, 'sp', axis=0, tiled=True)  33.4 us
    all_gather x1, blocking collectives, body(): lax.all_gather(value_weight, 'sp', axis=0, tiled=True)  31.4 us
    all_gather x1, blocking collectives, body(): shard_part = lax.all_gather(key_value, 'sp', axis=1, tiled=True)  29.7 us
    all_gather x1, blocking collectives, body(): lax.all_gather(local_state[:, seq_span - 1][None], 'sp', axis=0, tiled=True)  26.3 us
    all_gather x1, blocking collectives, body(): lax.all_gather(cum_decay[:, seq_span - 1][None], 'sp', axis=0, tiled=True)  26.1 us
    reduce_scatter x1, waiting for transfers between devices, body(): lax.psum_scatter(terms.reshape(row_count, pieces, out_cols).transpose(1,...  22.5 us
    slice x44, local copies, waits for them, and re-layouts, body(): lax.associative_scan(merge_state, (jnp.exp(log_decay), drive), axis=1)  11.2 us
    pad x24, local copies, waits for them, and re-layouts, body(): lax.associative_scan(merge_state, (jnp.exp(log_decay), drive), axis=1)  10.2 us
  transfers between devices with their start and end apart: 5, of which 2 were waited for; matrix products, arithmetic and copies ran while one was open for 24% of the time, Pallas kernels for 0%

commit v1 on v0

--- a/solution.py
+++ b/solution.py
@@ -109,7 +109,25 @@
         jnp.zeros((seq_count, kv_local, head_group * seq_span), jnp.float32),
         jnp.zeros((seq_count, kv_local, head_group * seq_span, head_dim), jnp.float32),
     )
-    shard_part = lax.all_gather(key_value, "sp", axis=1, tiled=True)
+    peers, mine, span_2 = (lax.axis_size("sp"), lax.axis_index("sp"), key_value.shape[1])
+    ahead = [(i, (i + 1) % peers) for i in range(peers)]
+    backward = [(i, (i - 1) % peers) for i in range(peers)]
+    shard_part = jnp.zeros(
+        (*key_value.shape[:1], peers * span_2, *key_value.shape[1 + 1 :]), key_value.dtype
+    )
+    shard_part = lax.dynamic_update_slice_in_dim(shard_part, key_value, mine * span_2, axis=1)
+    from_left = from_right = key_value
+    half = peers // 2
+    for step in range(1, half + 1):
+        from_left = lax.ppermute(from_left, "sp", ahead)
+        shard_part = lax.dynamic_update_slice_in_dim(
+            shard_part, from_left, (mine - step) % peers * span_2, axis=1
+        )
+        if step < peers - half:
+            from_right = lax.ppermute(from_right, "sp", backward)
+            shard_part = lax.dynamic_update_slice_in_dim(
+                shard_part, from_right, (mine + step) % peers * span_2, axis=1
+            )
     offset = jnp.int32(0)
     length = shard_part.shape[1]
     sub_size = block_length(length, seq_span)

time: 265 us -> 328 us (1.24)
  local copies, waits for them, and re-layouts: 35.4 us -> 90.6 us
  blocking collectives: 147 us -> 117 us
  other arithmetic: 24.8 us -> 38.4 us
  starting transfers between devices: 3.38 us -> 16.3 us
  waiting for transfers between devices: 25.4 us -> 32.6 us
    slice x44, local copies, waits for them, and re-layouts: 11.2 us -> 51.4 us  [body(): lax.associative_scan(merge_state, (jnp.exp(log_decay), drive), axis=1)]
    all_gather x1 -> x0, blocking collectives: 29.7 us -> none  [body(): shard_part = lax.all_gather(key_value, 'sp', axis=1, tiled=True)]
    ppermute x0 -> x7, starting transfers between devices: none -> 14.6 us  [the longest x3 12.3 us: body(): from_right = lax.ppermute(from_right, 'sp', backward)]
    sub x0 -> x2, local copies, waits for them, and re-layouts: none -> 9.52 us  [work(): scores.reshape(seq_count, kv_local, head_group, seq_span, sub_size)]
    add x13, other arithmetic: 4.34 us -> 13.8 us  [merge_state(): return (earlier[0] * later[0], later[0] * earlier[1] + later[1])]
    ppermute x0 -> x7, waiting for transfers between devices: none -> 8.25 us  [the longest x4 7.34 us: body(): from_left = lax.ppermute(from_left, 'sp', ahead)]
    dynamic_update_slice x0 -> x8, local copies, waits for them, and re-layouts: none -> 5.52 us  [the longest x4 2.61 us: body(): lax.dynamic_update_slice_in_dim(shard_part, from_left, (mine - step) % pe...]
    concatenate x11, other arithmetic: 3.16 us -> 7.84 us  [body(): lax.associative_scan(merge_state, (jnp.exp(log_decay), drive), axis=1)]
  transfers between devices with their start and end apart: 5 -> 12, of which waited for: 2 -> 7; matrix products, arithmetic and copies ran while one was open for 24% -> 41% of each run, Pallas kernels for 0% -> 0%
where the time goes in v1:
time: 328 us; the launch traced here: 324 us
  blocking collectives  117 us (36%)
  local copies, waits for them, and re-layouts  90.6 us (28%)
  other arithmetic  38.4 us (12%)
  waiting for transfers between devices  32.6 us (10%)
  starting transfers between devices  16.3 us (5%)
  matrix products  15.1 us (5%)
  between operations  13.9 us (4%)
    slice x44, local copies, waits for them, and re-layouts, body(): lax.associative_scan(merge_state, (jnp.exp(log_decay), drive), axis=1)  51.4 us
    all_gather x1, blocking collectives, body(): lax.all_gather(key_weight, 'sp', axis=0, tiled=True)  33.1 us
    all_gather x1, blocking collectives, body(): lax.all_gather(value_weight, 'sp', axis=0, tiled=True)  31.4 us
    all_gather x1, blocking collectives, body(): lax.all_gather(cum_decay[:, seq_span - 1][None], 'sp', axis=0, tiled=True)  26.1 us
    all_gather x1, blocking collectives, body(): lax.all_gather(local_state[:, seq_span - 1][None], 'sp', axis=0, tiled=True)  26.1 us
    reduce_scatter x1, waiting for transfers between devices, body(): lax.psum_scatter(terms.reshape(row_count, pieces, out_cols).transpose(1,...  22.9 us
    add x13, other arithmetic, merge_state(): return (earlier[0] * later[0], later[0] * earlier[1] + later[1])  13.8 us
    ppermute x3, starting transfers between devices, body(): from_right = lax.ppermute(from_right, 'sp', backward)  12.3 us
  transfers between devices with their start and end apart: 12, of which 7 were waited for; matrix products, arithmetic and copies ran while one was open for 41% of the time, Pallas kernels for 0%

profile of v1, /device:TPU:0, one launch (start us, length us, event | category | flops | bytes accessed | tf_op | source)
XLA Modules:
  0.0 323.7 jit_solution(13435449004433587643)
XLA Ops:
  8.1 1.5 multiply_reduce_fusion
  9.6 33.1 %all_gather.21 = bf16[2048,64]{0,1:T(8,128)(2,1)S(1)} all-gather(bf16[256,64]{0,1:T(8,128)(2,1)} %param.24), channel_id=1, replica_groups=mesh['sp'=8,'tp'=4] {'sp'}, dimensions={0}, use_global_device_ids=true | all-gather | bytes 294912 | tf_op jit(solution)/shard_map/all_gather | solution.py:76
  42.7 31.4 %all_gather.22 = bf16[2048,64]{0,1:T(8,128)(2,1)S(1)} all-gather(bf16[256,64]{0,1:T(8,128)(2,1)} %param.25), channel_id=1, replica_groups=mesh['sp'=8,'tp'=4] {'sp'}, dimensions={0}, use_global_device_ids=true | all-gather | bytes 294912 | tf_op jit(solution)/shard_map/all_gather | solution.py:77
  74.1 1.5 fusion.20
  76.6 1.6 collective-permute-start
  78.3 3.1 collective-permute-start.1
  85.2 4.2 %collective-permute-start.3 = (bf16[2,128,128]{1,2,0:T(8,128)(2,1)S(1)}, bf16[2,128,128]{1,2,0:T(8,128)(2,1)}, u32[]{:S(2)}, u32[]{:S(2)}) collective-permute-start(bf16[2,128,128]{1,2,0:T(8,128)(2,1)S(1)} %collective-permute-done.1), channel_id=1, source_target_pairs={{0,28},{4,0},{8,4},{12,8},{16,12},{20,16},{24,20},{28,24},{1,29},{... | collective-permute-start | bytes 196616 | tf_op jit(solution)/shard_map/ppermute | solution.py:127
  91.5 5.0 %collective-permute-start.5 = (bf16[2,128,128]{1,2,0:T(8,128)(2,1)}, bf16[2,128,128]{1,2,0:T(8,128)(2,1)}, u32[]{:S(2)}, u32[]{:S(2)}) collective-permute-start(bf16[2,128,128]{1,2,0:T(8,128)(2,1)} %collective-permute-done.3), channel_id=1, source_target_pairs={{0,28},{4,0},{8,4},{12,8},{16,12},{20,16},{24,20},{28,24},{1,29},{... | collective-permute-start | bytes 196616 | tf_op jit(solution)/shard_map/ppermute | solution.py:127
  96.5 1.9 collective-permute-done.4
  98.5 1.5 copy.58
  100.0 1.7 multiply_reduce_fusion.1
  102.6 3.1 collective-permute-done.6
  105.7 24.2 %conditional.1 = ((f32[2,1,512]{2,0,1:T(2,128)S(1)}, f32[2,1,512,64]{2,3,0,1:T(8,128)S(1)})) conditional(s32[]{:T(128)} %convert_element_type.126, (f32[2,1,512]{2,0,1:T(2,128)S(1)}, f32[2,1,512,64]{2,3,0,1:T(8,128)S(1)}) %tuple.93, (s32[]{:T(128)}, s32[4,128]{1,0:T(4,128)S(1)}, bf16[2,128,128]{1,2,0:T(8,128)(2,1)S(1)}, s32[]{:T(128)}, ...), branch_computations={%region_3.4_spmd, %region_4.7_spmd.clone.clone} | conditional | flops 278534784 | bytes 39890236 | solution.py:176
  114.6 3.9 %sub.101 = f32[2,4,128,1024]{2,1,3,0:T(4,128)} broadcast(f32[2,4,1024]{1,2,0:T(8,128)S(1)} %copy.81), dimensions={0,1,3} | broadcast | bytes 4227072 | tf_op jit(solution)/shard_map/while/body/eval_jaxpr/cond/branch_1_fun/sub | solution.py:154
  118.6 5.6 %sub.102 = f32[2,512,1024]{1,2,0:T(8,128)} reshape(f32[2,4,128,1024]{2,1,3,0:T(4,128)} %sub.101) | data formatting | bytes 8388608 | tf_op jit(solution)/shard_map/while/body/eval_jaxpr/cond/branch_1_fun/sub | solution.py:154
  125.1 3.4 %fusion.75 = (f32[2,512]{1,0:T(2,128)S(1)}, f32[2,512,1024]{1,2,0:T(8,128)S(1)}) fusion(f32[2,512,1024]{1,2,0:T(8,128)} %sub.102, f32[2,512]{1,0:T(2,128)S(1)} %bitcast.180, bf16[2,512,64]{1,2,0:T(8,128)(2,1)S(1)} %reshape.403, bf16[2,1024,128]{1,2,0:T(8,128)(2,1)S(1)} %copy-done.4, pred[512,1024]{0,1:T(8,128)(4,1)S(1)} %copy-done.2), kind=kOutput, calls=%fused_computation.172 | convolution fusion | flops 139459584 | bytes 9314304 | tf_op jit(solution)/shard_map/while/body/eval_jaxpr/cond/branch_1_fun/bhqd,bkhd->bhqk/dot_general | solution.py:148
  130.6 1.7 convolution_convert_fusion
  132.3 1.5 collective-permute-start.7
  139.2 2.0 convert_multiply_fusion
  141.2 1.6 slice.320
  142.8 1.6 slice.321
  145.8 1.8 multiply_add_fusion.1
  147.6 1.5 slice.326
  149.1 1.5 slice.327
  151.9 1.6 multiply_add_fusion.2
  153.5 1.5 slice.332
  155.0 1.4 slice.333
  156.4 1.4 slice.331
  157.9 1.4 slice.335
  159.3 1.4 multiply_add_fusion.3
  189.2 1.4 slice.330
  190.6 1.5 slice.363
  195.3 1.5 slice.365
  199.4 1.6 slice.367
  212.5 1.5 fusion.55
  215.6 1.5 pad_maximum_fusion.4
  217.1 2.1 pad.129
  219.8 1.6 add.516
  221.4 1.7 fusion.51
  223.2 2.3 pad.118
  226.4 1.4 pad.131
  227.8 2.3 pad.132
  231.6 26.1 %all-gather = f32[16,1,256]{2,1,0:T(1,128)S(1)} all-gather(f32[2,1,256]{2,1,0:T(1,128)S(1)} %slice_add_fusion.4), channel_id=2, replica_groups=mesh['sp'=8,'tp'=4] {'sp'}, dimensions={0}, use_global_device_ids=true | all-gather | bytes 18432 | tf_op jit(solution)/shard_map/all_gather | solution.py:217
  257.7 26.1 %all-gather.1 = f32[16,1,256]{2,1,0:T(1,128)S(1)} all-gather(f32[2,1,256]{2,1,0:T(1,128)S(1)} %slice_add_fusion.3), channel_id=3, replica_groups=mesh['sp'=8,'tp'=4] {'sp'}, dimensions={0}, use_global_device_ids=true | all-gather | bytes 18432 | tf_op jit(solution)/shard_map/all_gather | solution.py:216
  284.3 3.0 fusion.80
  287.3 1.8 copy.71
  291.5 1.7 fusion.18
  294.3 22.9 %reduce-scatter.2.cloned.1.call-done = bf16[256,512]{1,0:T(8,128)(2,1)} async-done(((bf16[1024,512]{1,0:T(8,128)(2,1)}), bf16[256,512]{1,0:T(8,128)(2,1)}) %reduce-scatter.2.cloned.1.call-update) | async-done | bytes 262160 | tf_op jit(solution)/shard_map/reduce_scatter | solution.py:239
  (222 shorter events, 82.9 us)
Async XLA Ops:
  6.5 128.0 %copy-start = (bf16[256,2048]{1,0:T(8,128)(2,1)S(1)}, bf16[256,2048]{1,0:T(8,128)(2,1)}, u32[]{:S(2)}) copy-start(bf16[256,2048]{1,0:T(8,128)(2,1)} %param.38) | copy-start | bytes 3145732
  6.5 75.0 %copy-start.1 = (bf16[2,128,2048]{2,1,0:T(8,128)(2,1)S(1)}, bf16[2,128,2048]{2,1,0:T(8,128)(2,1)}, u32[]{:S(2)}) copy-start(bf16[2,128,2048]{2,1,0:T(8,128)(2,1)} %param.21) | copy-start | bytes 3145732
  6.5 75.0 %copy-start.8 = (f32[2048]{0:T(1024)S(1)}, f32[2048]{0:T(1024)}, u32[]{:S(2)}) copy-start(f32[2048]{0:T(1024)} %param.22) | copy-start | bytes 24580
  6.5 70.0 %copy-start.18 = (f32[64]{0:T(128)S(1)}, f32[64]{0:T(128)}, u32[]{:S(2)}) copy-start(f32[64]{0:T(128)} %param.27) | copy-start | bytes 772
  6.5 91.9 %all-gather.6.cloned.1.call-start = ((), (), s32[]{:S(2)}) async-start(), calls=%async_computation.1 | async-start | bytes 1179648 | tf_op jit(solution)/shard_map/all_gather | solution.py:75
  7.3 123.3 %all-gather.8.cloned.1.call-start = ((), (), s32[]{:S(2)}) async-start(), calls=%async_computation.2 | async-start | bytes 1179648 | tf_op jit(solution)/shard_map/all_gather | solution.py:78
  8.0 76.4 %copy-start.11 = (bf16[4,256]{1,0:T(4,128)(2,1)S(1)}, bf16[4,256]{1,0:T(4,128)(2,1)}, u32[]{:S(2)}) copy-start(bf16[4,256]{1,0:T(4,128)(2,1)} %param.31) | copy-start | bytes 6148
  8.0 82.7 %copy-start.17 = (f32[256]{0:T(256)S(1)}, f32[256]{0:T(256)}, u32[]{:S(2)}) copy-start(f32[256]{0:T(256)} %param.34) | copy-start | bytes 3076
  8.0 276.2 %all-gather.10.cloned.1.call-start = ((), (), s32[]{:S(2)}) async-start(), calls=%async_computation.3 | async-start | bytes 1179648 | tf_op jit(solution)/shard_map/all_gather | solution.py:79
  76.5 25.2 %copy-start.19 = (f32[64]{0:T(128)S(1)}, f32[64]{0:T(128)}, u32[]{:S(2)}) copy-start(f32[64]{0:T(128)} %param.26) | copy-start | bytes 772
  76.6 7.0 %collective-permute-start = (bf16[2,128,128]{1,2,0:T(8,128)(2,1)S(1)}, bf16[2,128,128]{1,2,0:T(8,128)(2,1)S(1)}, u32[]{:S(2)}, u32[]{:S(2)}) collective-permute-start(bf16[2,128,128]{1,2,0:T(8,128)(2,1)S(1)} %bitcast_dynamic-update-slice_fusion), channel_id=1, source_target_pairs={{0,4},{4,8},{8,12},{12,16},{16,20},{20,24},{24,28},{28,0},{1,5},{5... | collective-permute-start | bytes 196616 | tf_op jit(solution)/shard_map/ppermute | solution.py:122
  78.3 6.9 %collective-permute-start.1 = (bf16[2,128,128]{1,2,0:T(8,128)(2,1)S(1)}, bf16[2,128,128]{1,2,0:T(8,128)(2,1)S(1)}, u32[]{:S(2)}, u32[]{:S(2)}) collective-permute-start(bf16[2,128,128]{1,2,0:T(8,128)(2,1)S(1)} %bitcast_dynamic-update-slice_fusion), channel_id=1, source_target_pairs={{0,28},{4,0},{8,4},{12,8},{16,12},{20,16},{24,20},{28,24},{1,29},{... | collective-permute-start | bytes 196616 | tf_op jit(solution)/shard_map/ppermute | solution.py:127
  81.4 235.8 %reduce-scatter.2.cloned.1.call-start = ((), (), s32[]{:S(2)}) async-start(), calls=%async_computation.4 | async-start | bytes 1310720 | tf_op jit(solution)/shard_map/reduce_scatter | solution.py:239
  83.7 7.1 %collective-permute-start.2 = (bf16[2,128,128]{1,2,0:T(8,128)(2,1)S(1)}, bf16[2,128,128]{1,2,0:T(8,128)(2,1)S(1)}, u32[]{:S(2)}, u32[]{:S(2)}) collective-permute-start(bf16[2,128,128]{1,2,0:T(8,128)(2,1)S(1)} %collective-permute-done), channel_id=1, source_target_pairs={{0,4},{4,8},{8,12},{12,16},{16,20},{20,24},{24,28},{28,0},{1,5},{5... | collective-permute-start | bytes 196616 | tf_op jit(solution)/shard_map/ppermute | solution.py:122
  85.2 13.3 %copy-start.6 = (bf16[2,128,128]{1,2,0:T(8,128)(2,1)}, bf16[2,128,128]{1,2,0:T(8,128)(2,1)S(1)}, u32[]{:S(2)}) copy-start(bf16[2,128,128]{1,2,0:T(8,128)(2,1)S(1)} %collective-permute-done.1) | copy-start | bytes 196612
  85.2 6.3 %collective-permute-start.3 = (bf16[2,128,128]{1,2,0:T(8,128)(2,1)S(1)}, bf16[2,128,128]{1,2,0:T(8,128)(2,1)}, u32[]{:S(2)}, u32[]{:S(2)}) collective-permute-start(bf16[2,128,128]{1,2,0:T(8,128)(2,1)S(1)} %collective-permute-done.1), channel_id=1, source_target_pairs={{0,28},{4,0},{8,4},{12,8},{16,12},{20,16},{24,20},{28,24},{1,29},{... | collective-permute-start | bytes 196616 | tf_op jit(solution)/shard_map/ppermute | solution.py:127
  90.7 7.7 %copy-start.7 = (bf16[2,128,128]{1,2,0:T(8,128)(2,1)}, bf16[2,128,128]{1,2,0:T(8,128)(2,1)S(1)}, u32[]{:S(2)}) copy-start(bf16[2,128,128]{1,2,0:T(8,128)(2,1)S(1)} %collective-permute-done.2) | copy-start | bytes 196612
  90.8 7.7 %collective-permute-start.4 = (bf16[2,128,128]{1,2,0:T(8,128)(2,1)S(1)}, bf16[2,128,128]{1,2,0:T(8,128)(2,1)}, u32[]{:S(2)}, u32[]{:S(2)}) collective-permute-start(bf16[2,128,128]{1,2,0:T(8,128)(2,1)S(1)} %collective-permute-done.2), channel_id=1, source_target_pairs={{0,4},{4,8},{8,12},{12,16},{16,20},{20,24},{24,28},{28,0},{1,5},{5... | collective-permute-start | bytes 196616 | tf_op jit(solution)/shard_map/ppermute | solution.py:122
  91.5 11.1 %collective-permute-start.5 = (bf16[2,128,128]{1,2,0:T(8,128)(2,1)}, bf16[2,128,128]{1,2,0:T(8,128)(2,1)}, u32[]{:S(2)}, u32[]{:S(2)}) collective-permute-start(bf16[2,128,128]{1,2,0:T(8,128)(2,1)} %collective-permute-done.3), channel_id=1, source_target_pairs={{0,28},{4,0},{8,4},{12,8},{16,12},{20,16},{24,20},{28,24},{1,29},{... | collective-permute-start | bytes 196616 | tf_op jit(solution)/shard_map/ppermute | solution.py:127
  98.5 7.3 %collective-permute-start.6 = (bf16[2,128,128]{1,2,0:T(8,128)(2,1)}, bf16[2,128,128]{1,2,0:T(8,128)(2,1)}, u32[]{:S(2)}, u32[]{:S(2)}) collective-permute-start(bf16[2,128,128]{1,2,0:T(8,128)(2,1)} %collective-permute-done.4), channel_id=1, source_target_pairs={{0,4},{4,8},{8,12},{12,16},{16,20},{20,24},{24,28},{28,0},{1,5},{5... | collective-permute-start | bytes 196616 | tf_op jit(solution)/shard_map/ppermute | solution.py:122
  111.5 0.8 copy-start.3
  118.6 6.5 %copy-start.2 = (pred[512,1024]{0,1:T(8,128)(4,1)S(1)}, pred[512,1024]{0,1:T(8,128)(4,1)}, u32[]{:S(2)}) copy-start(pred[512,1024]{0,1:T(8,128)(4,1)} %iota_compare_fusion) | copy-start | bytes 1572868 | tf_op jit(solution)/shard_map/while/body/eval_jaxpr/cond
  118.6 6.5 %copy-start.4 = (bf16[2,1024,128]{1,2,0:T(8,128)(2,1)S(1)}, bf16[2,1024,128]{1,2,0:T(8,128)(2,1)}, u32[]{:S(2)}) copy-start(bf16[2,1024,128]{1,2,0:T(8,128)(2,1)} %copy-done.3) | copy-start | bytes 1572868 | tf_op jit(solution)/shard_map/while/body/eval_jaxpr/cond
  130.0 5.1 %copy-start.12 = (f32[1,256]{1,0:T(1,128)S(1)}, f32[1,256]{1,0:T(1,128)}, u32[]{:S(2)}) copy-start(f32[1,256]{1,0:T(1,128)} %get-tuple-element.948) | copy-start | bytes 3076
  130.0 5.1 %copy-start.13 = (f32[1,256]{1,0:T(1,128)S(1)}, f32[1,256]{1,0:T(1,128)}, u32[]{:S(2)}) copy-start(f32[1,256]{1,0:T(1,128)} %get-tuple-element.949) | copy-start | bytes 3076
  130.0 5.1 %copy-start.14 = (f32[1,256]{1,0:T(1,128)S(1)}, f32[1,256]{1,0:T(1,128)}, u32[]{:S(2)}) copy-start(f32[1,256]{1,0:T(1,128)} %get-tuple-element.950) | copy-start | bytes 3076
  130.0 5.1 %copy-start.15 = (f32[1,256]{1,0:T(1,128)S(1)}, f32[1,256]{1,0:T(1,128)}, u32[]{:S(2)}) copy-start(f32[1,256]{1,0:T(1,128)} %get-tuple-element.951) | copy-start | bytes 3076
  130.0 6.0 %copy-start.20 = (bf16[4,64,64]{2,1,0:T(8,128)(2,1)S(1)}, bf16[4,64,64]{2,1,0:T(8,128)(2,1)}, u32[]{:S(2)}) copy-start(bf16[4,64,64]{2,1,0:T(8,128)(2,1)} %param.32) | copy-start | bytes 98308
  132.3 2.8 collective-permute-start.7
  135.4 0.7 copy-start.5
  208.1 15.0 %copy-start.10 = (f32[2,1,256]{2,1,0:T(1,128)S(1)}, f32[2,1,256]{2,1,0:T(1,128)}, u32[]{:S(2)}) copy-start(f32[2,1,256]{2,1,0:T(1,128)} %slice.414) | copy-start | bytes 6148
  208.1 17.4 %copy-start.9 = (f32[2,1,256]{2,1,0:T(1,128)S(1)}, f32[2,1,256]{2,1,0:T(1,128)}, u32[]{:S(2)}) copy-start(f32[2,1,256]{2,1,0:T(1,128)} %slice.437) | copy-start | bytes 6148
  223.1 68.3 %copy-start.16 = (f32[256]{0:T(256)S(1)}, f32[256]{0:T(256)}, u32[]{:S(2)}) copy-start(f32[256]{0:T(256)} %param.37) | copy-start | bytes 3076
Sparse Core Ops, SparseCore 0:
  9.5 43.3 all-gather.5
  55.0 41.0 all-gather.7
  98.3 40.6 all-gather.9
  294.4 22.7 reduce-scatter.1
